TPU v7x, 128 devices: a whole 4x4x4 slice. The times are simulated.
128 devices in a mesh: ep: 64 (over z, y, x), tp: 2 (over core).
Axes of the slice: x: 4, y: 4, z: 4, core: 2. Of those that a mesh axis runs over, the one named last changes fastest.
Arguments:
- tokens: bfloat16 [2048, 1024], P(('ep', 'tp')), may hold values from -6 to 6
- lengths: int32 [2048], P(('ep', 'tp')), may hold values from 1 to 1024
- cache_latent: bfloat16 [2048, 1024, 256], P(('ep', 'tp')), may hold values from -700 to 700
- cache_rope: bfloat16 [2048, 32, 1024], P(('ep', 'tp')), may hold values from -6 to 6
- attn_gain: bfloat16 [1024], replicated, may hold values from 0.099609375 to 1.8984375
- w_dq: bfloat16 [1024, 512], replicated, may hold values from -0.1875 to 0.1875
- q_gain: bfloat16 [512], replicated, may hold values from 0.099609375 to 1.8984375
- w_q_nope: bfloat16 [512, 1024], replicated, may hold values from -0.25 to 0.25
- w_q_rope: bfloat16 [512, 512], replicated, may hold values from -0.25 to 0.25
- w_dkv: bfloat16 [1024, 256], replicated, may hold values from -0.1875 to 0.1875
- kv_gain: bfloat16 [256], replicated, may hold values from 0.099609375 to 1.8984375
- w_krope: bfloat16 [1024, 32], replicated, may hold values from -0.1875 to 0.1875
- w_uk: bfloat16 [256, 1024], replicated, may hold values from -0.75 to 0.75
- w_uv: bfloat16 [256, 1024], replicated, may hold values from -0.375 to 0.375
- w_o: bfloat16 [1024, 1024], replicated, may hold values from -0.1875 to 0.1875
- post_gain: bfloat16 [1024], replicated, may hold values from 0.099609375 to 1.8984375
- moe_gain: bfloat16 [1024], replicated, may hold values from 0.099609375 to 1.8984375
- routes: int32 [2048, 4], P(('ep', 'tp')), may hold values from 0 to 63, all different within a row; in each aligned block of 16 rows (0 to 15, 16 to 31, ...) at most 3 rows name the same one
- route_scores: float32 [2048, 4], P(('ep', 'tp')), may hold values from 0.05 to 1
- expert_gate: bfloat16 [64, 1024, 512], P('ep', None, 'tp'), may hold values from -0.1875 to 0.1875
- expert_up: bfloat16 [64, 1024, 512], P('ep', None, 'tp'), may hold values from -0.1875 to 0.1875
- expert_down: bfloat16 [64, 512, 1024], P('ep', 'tp'), may hold values from -0.25 to 0.25
- shared_gate: bfloat16 [1024, 512], replicated, may hold values from -0.1875 to 0.1875
- shared_up: bfloat16 [1024, 512], replicated, may hold values from -0.1875 to 0.1875
- shared_down: bfloat16 [512, 1024], replicated, may hold values from -0.25 to 0.25
- dense_vec: bfloat16 [1024], replicated, may hold values from -0.1875 to 0.1875
- dense_w_gate: bfloat16 [1024, 8192], P(None, ('ep', 'tp')), may hold values from -0.1875 to 0.1875
- dense_w_up: bfloat16 [1024, 8192], P(None, ('ep', 'tp')), may hold values from -0.1875 to 0.1875
- dense_w_down: bfloat16 [8192, 1024], P(('ep', 'tp')), may hold values from -0.25 to 0.25
- out_gain: bfloat16 [1024], replicated, may hold values from 0.099609375 to 1.8984375
Outputs:
- hidden_out: bfloat16 [2048, 1024], P(('ep', 'tp'))
- new_latent: bfloat16 [2048, 256], P(('ep', 'tp'))
Inputs may be any that keep to these rules, and one draw needn't show every extreme that they name: `routes`: each row names 4 different experts. In the 16 rows of one device no expert is named more than 3 times, a bound that some block reaches in some devices' rows.
All inputs are finite; a program needn't handle non-finite values.
Results may differ from a plain program's by a relative error of at most 0.011.
The roundings to bfloat16 on the way count: a program that leaves them out, or rounds other values in their place, can miss the bound.
Values may be sent and summed in bfloat16 or wider, within the bound.
A program may use at most 128 MiB of HBM per device.

v0:
```python
from functools import partial

import jax
import jax.numpy as jnp
from jax import lax
from jax.sharding import Mesh
from jax.sharding import PartitionSpec as P

HEADS = 16
NOPE = 64
ROPE = 32
VDIM = 64
EP = ("ep_0", "ep_1", "ep_2")
EP_TP = ("ep_0", "ep_1", "ep_2", "tp")


eps = 1e-06
rope_base = 10000.0
routed_scale = 2.5


def from_everyone(shard, axis):
    devices = lax.axis_size(axis)
    return lax.all_to_all(
        jnp.broadcast_to(shard[None], (devices, *shard.shape)), axis, 0, 0, tiled=True
    )


def laid_out(tiles, dim):
    tiles = jnp.moveaxis(tiles, 0, dim)
    dims = tiles.shape
    return tiles.reshape(*dims[:dim], dims[dim] * dims[dim + 1], *dims[dim + 2 :])


def whole_of(shard, axes, dim):
    far, near = axes
    initial = from_everyone(shard, far)
    tiles = jnp.swapaxes(from_everyone(initial, near), 0, 1)
    return laid_out(tiles.reshape(-1, *shard.shape), dim)


def in_blocks(shard, dim, devices):
    dims = shard.shape
    tiles = shard.reshape(*dims[:dim], devices, dims[dim] // devices, *dims[dim + 1 :])
    return jnp.moveaxis(tiles, dim, 0)


def sum_at_owner(shard, axis, dim):
    devices = lax.axis_size(axis)
    tiles = lax.all_to_all(in_blocks(shard, dim, devices), axis, 0, 0, tiled=True)
    return jnp.sum(tiles.astype(jnp.float32), axis=0)


def sum_in_two_steps(shard, axes, dim):
    far, near = axes
    tiles = in_blocks(shard, dim, lax.axis_size(far))
    nearer = sum_at_owner(tiles, near, dim + 1)
    arrived = lax.all_to_all(
        nearer.astype(jnp.bfloat16), far, split_axis=0, concat_axis=0, tiled=True
    )
    return arrived.astype(jnp.float32).sum(axis=0)


def rms_scale(value, gain):
    value = value.astype(jnp.float32)
    inverse = lax.rsqrt(jnp.mean(value * value, axis=-1, keepdims=True) + eps)
    return value * inverse * gain.astype(jnp.float32)


def angles(lengths, rope_dim):
    half = rope_dim // 2
    freqs = rope_base ** (-jnp.arange(half, dtype=jnp.float32) / half)
    angle = lengths.astype(jnp.float32)[:, None] * freqs[None, :]
    return (jnp.cos(angle), jnp.sin(angle))


def rotate(value, cosine, sine):
    half = value.shape[-1] // 2
    first, second = (value[..., :half], value[..., half:])
    return jnp.concatenate(
        [first * cosine - second * sine, second * cosine + first * sine], axis=-1
    )


def slot_table(ids, scores, experts, cap):
    rows, top = ids.shape
    norm = scores / jnp.sum(scores, axis=1, keepdims=True) * routed_scale
    flat = ids.reshape(-1)
    onehot = (flat[:, None] == jnp.arange(experts, dtype=jnp.int32)[None, :]).astype(jnp.int32)
    rank = jnp.cumsum(onehot, axis=0) - 1
    hit = onehot[:, :, None] * (
        rank[:, :, None] == jnp.arange(cap, dtype=jnp.int32)[None, None, :]
    ).astype(jnp.int32)
    owner = jnp.arange(rows * top, dtype=jnp.int32) // top
    token_of = jnp.sum(hit * owner[:, None, None], axis=0)
    weight_of = jnp.sum(hit.astype(jnp.float32) * norm.reshape(-1)[:, None, None], axis=0)
    return (token_of, weight_of)


def attention(
    tokens,
    lengths,
    latent,
    rope_keys,
    attn_gain,
    w_dq,
    q_gain,
    w_q_nope,
    w_q_rope,
    w_dkv,
    kv_gain,
    w_krope,
    w_uk,
    w_uv,
    w_o,
    post_gain,
):
    f32 = jnp.float32
    bf16 = jnp.bfloat16
    seqs = tokens.shape[0]
    latent_width = w_dkv.shape[1]
    normed = rms_scale(tokens, attn_gain).astype(bf16)
    q_normed = rms_scale(jnp.dot(normed, w_dq, preferred_element_type=f32), q_gain).astype(bf16)
    q_nope = (
        jnp.dot(q_normed, w_q_nope, preferred_element_type=f32)
        .astype(bf16)
        .reshape(seqs, HEADS, NOPE)
    )
    cosine, sine = angles(lengths, ROPE)
    q_raw = jnp.dot(q_normed, w_q_rope, preferred_element_type=f32).reshape(seqs, HEADS, ROPE)
    q_rot = rotate(q_raw, cosine[:, None, :], sine[:, None, :]).astype(bf16)
    new_latent = rms_scale(jnp.dot(normed, w_dkv, preferred_element_type=f32), kv_gain).astype(bf16)
    new_rope = rotate(jnp.dot(normed, w_krope, preferred_element_type=f32), cosine, sine).astype(
        bf16
    )
    query_lat = jnp.einsum(
        "shn,chn->shc", q_nope, w_uk.reshape(latent_width, HEADS, NOPE), preferred_element_type=f32
    ).astype(bf16)
    scale = (NOPE + ROPE) ** (-0.5)
    past = jnp.einsum("shc,slc->shl", query_lat, latent, preferred_element_type=f32)
    past = (past + jnp.einsum("shr,srl->shl", q_rot, rope_keys, preferred_element_type=f32)) * scale
    own = jnp.einsum("shc,sc->sh", query_lat, new_latent, preferred_element_type=f32)
    own = (own + jnp.einsum("shr,sr->sh", q_rot, new_rope, preferred_element_type=f32)) * scale
    valid = jnp.arange(latent.shape[1], dtype=jnp.int32)[None, None, :] < lengths[:, None, None]
    top = jnp.maximum(jnp.max(jnp.where(valid, past, -1e30), axis=-1), own)
    past_weight = jnp.where(valid, jnp.exp(past - top[..., None]), 0.0)
    own_weight = jnp.exp(own - top)
    total = jnp.sum(past_weight, axis=-1) + own_weight
    past_prob = (past_weight / total[..., None]).astype(bf16)
    own_prob = (own_weight / total).astype(bf16)
    mixed = jnp.einsum("shl,slc->shc", past_prob, latent, preferred_element_type=f32)
    mixed = (mixed + own_prob.astype(f32)[..., None] * new_latent.astype(f32)[:, None, :]).astype(
        bf16
    )
    head_out = jnp.einsum(
        "shc,chv->shv", mixed, w_uv.reshape(latent_width, HEADS, VDIM), preferred_element_type=f32
    ).astype(bf16)
    attn_out = jnp.dot(head_out.reshape(seqs, HEADS * VDIM), w_o, preferred_element_type=f32)
    first = (tokens.astype(f32) + rms_scale(attn_out, post_gain)).astype(bf16)
    return (first, new_latent)


def expert_apply(rows, gate_w, up_w, down_w):
    hidden_gate = jnp.einsum("necd,edf->necf", rows, gate_w, preferred_element_type=jnp.float32)
    hidden_up = jnp.einsum("necd,edf->necf", rows, up_w, preferred_element_type=jnp.float32)
    act = (jax.nn.silu(hidden_gate) * hidden_up).astype(jnp.bfloat16)
    return (
        jnp.einsum("necf,efd->necd", act, down_w, preferred_element_type=jnp.float32)
        .astype(jnp.bfloat16)
        .astype(jnp.float32)
    )


def dense_partial(rows, w_gate, w_up, w_down):
    act = (
        jax.nn.silu(jnp.dot(rows, w_gate, preferred_element_type=jnp.float32))
        * jnp.dot(rows, w_up, preferred_element_type=jnp.float32)
    ).astype(jnp.bfloat16)
    return jnp.dot(act, w_down, preferred_element_type=jnp.float32)


def shards(
    tokens,
    lengths,
    cache_latent,
    cache_rope,
    attn_gain,
    w_dq,
    q_gain,
    w_q_nope,
    w_q_rope,
    w_dkv,
    kv_gain,
    w_krope,
    w_uk,
    w_uv,
    w_o,
    post_gain,
    moe_gain,
    routes,
    route_scores,
    expert_gate,
    expert_up,
    expert_down,
    shared_gate,
    shared_up,
    shared_down,
    dense_vec,
    dense_w_gate,
    dense_w_up,
    dense_w_down,
    out_gain,
):
    f32 = jnp.float32
    bf16 = jnp.bfloat16
    first, new_latent = attention(
        tokens,
        lengths,
        cache_latent,
        cache_rope,
        attn_gain,
        w_dq,
        q_gain,
        w_q_nope,
        w_q_rope,
        w_dkv,
        kv_gain,
        w_krope,
        w_uk,
        w_uv,
        w_o,
        post_gain,
    )
    moe_in = rms_scale(first, moe_gain).astype(bf16)
    seqs, width = moe_in.shape
    shared_act = (
        jax.nn.silu(jnp.dot(moe_in, shared_gate, preferred_element_type=f32))
        * jnp.dot(moe_in, shared_up, preferred_element_type=f32)
    ).astype(bf16)
    shared_out = jnp.dot(shared_act, shared_down, preferred_element_type=f32)
    ep_count = lax.axis_size(EP)
    exp_dev = expert_gate.shape[0]
    experts = exp_dev * ep_count
    top = routes.shape[1]
    cap = seqs * top // experts + 2
    every_rows = lax.all_gather(moe_in, EP_TP, axis=0, tiled=True)
    all_ids = whole_of(routes, (("ep_0", "ep_1", "ep_2"), "tp"), 0)
    all_scores = whole_of(route_scores, (("ep_0", "ep_1", "ep_2"), "tp"), 0)
    blocks = all_ids.shape[0] // seqs
    token_all, weight_all = jax.vmap(partial(slot_table, experts=experts, cap=cap))(
        all_ids.reshape(blocks, seqs, top), all_scores.reshape(blocks, seqs, top)
    )
    first_expert = lax.axis_index(EP) * exp_dev
    mine_token = lax.dynamic_slice_in_dim(token_all, first_expert, exp_dev, 1)
    mine_weight = lax.dynamic_slice_in_dim(weight_all, first_expert, exp_dev, 1)
    where_rows = mine_token + (jnp.arange(blocks, dtype=jnp.int32) * seqs)[:, None, None]
    picked = every_rows[where_rows]
    weighted = expert_apply(picked, expert_gate, expert_up, expert_down) * mine_weight[..., None]
    routed_all = (
        jnp.zeros(every_rows.shape, f32).at[where_rows.reshape(-1)].add(weighted.reshape(-1, width))
    )
    gate_all = jax.nn.sigmoid(jnp.dot(every_rows, dense_vec, preferred_element_type=f32))
    mixture = (
        sum_in_two_steps(
            (
                gate_all[:, None]
                * dense_partial(every_rows, dense_w_gate, dense_w_up, dense_w_down)
                + routed_all
            ).astype(jnp.bfloat16),
            (("ep_0", "ep_1", "ep_2"), "tp"),
            0,
        )
        + shared_out
    )
    hidden_out = (first.astype(f32) + rms_scale(mixture, out_gain)).astype(bf16)
    return (hidden_out, new_latent)


def solution(mesh):
    finer = Mesh(mesh.devices.reshape(4, 4, 4, mesh.shape["tp"]), ("ep_0", "ep_1", "ep_2", "tp"))
    placed = (
        P(EP_TP, None),
        P(EP_TP),
        P(EP_TP, None, None),
        P(EP_TP, None, None),
        P(),
        P(),
        P(),
        P(),
        P(),
        P(),
        P(),
        P(),
        P(),
        P(),
        P(),
        P(),
        P(),
        P(EP_TP, None),
        P(EP_TP, None),
        P(EP, None, "tp"),
        P(EP, None, "tp"),
        P(EP, "tp", None),
        P(),
        P(),
        P(),
        P(),
        P(None, EP_TP),
        P(None, EP_TP),
        P(EP_TP, None),
        P(),
    )
    return jax.shard_map(
        shards,
        mesh=finer,
        in_specs=placed,
        out_specs=(P(EP_TP, None), P(EP_TP, None)),
        check_vma=False,
    )
```

profile of v0, /device:TPU:1, one launch (start us, length us, event | category | flops | bytes accessed | tf_op | source)
XLA Modules:
  0.0 209.5 jit_solution(3018317602012080033)
XLA Ops:
  7.3 0.8 convert_element_type.135
  8.1 0.7 iota_compare_fusion.2
  8.8 0.7 convert_element_type.128
  9.5 0.9 fusion.46
  10.4 1.6 multiply_reduce_fusion.2
  12.0 0.7 convert_element_type.130
  12.7 1.2 fusion.75
  14.1 1.1 fusion.76
  15.1 1.5 convolution_convert_fusion.3
  16.8 1.2 copy.135
  18.3 1.6 fusion.63
  20.2 1.4 multiply_reduce_fusion.3
  22.0 5.8 %select_reduce_fusion = (f32[16,16]{1,0:T(8,128)S(1)}, f32[16,16,1024]{2,1,0:T(8,128)S(1)}) fusion(pred[16,1024]{1,0:T(8,128)(4,1)S(1)} %iota_compare_fusion.2, f32[16,16,1024]{2,1,0:T(8,128)S(1)} %fusion.63, bf16[16,1024,256]{2,1,0:T(8,128)(2,1)} %param.32, bf16[16,16,256]{2,0,1:T(8,128)(2,1)S(1)} %fusion.11), kind=kOutput, calls=%fused_computation.38 | convolution fusion | flops 135266048 | bytes 10634240 | tf_op jit(solution)/shard_map/shc,slc->shl/dot_general | solution.py:140
  28.2 2.0 copy.138
  30.2 4.7 %fusion.9 = bf16[16,16,256]{2,1,0:T(8,128)(2,1)S(1)} fusion(bf16[16,1024,256]{2,1,0:T(8,128)(2,1)} %param.32, f32[16,16,1024]{2,1,0:T(8,128)S(1)} %get-tuple-element.19, f32[16,16]{1,0:T(8,128)S(1)} %get-tuple-element.11, f32[16,16]{1,0:T(8,128)S(1)} %fusion.66, pred[16,1024]{1,0:T(8,128)(4,1)S(1)} %iota_compare_fusion.2, ...), kind=kOutput, calls=%fused_computation.26 | convolution fusion | flops 135462912 | bytes 9604096 | tf_op jit(solution)/shard_map/shl,slc->shc/dot_general | solution.py:151
  36.1 0.7 fusion.52
  37.5 12.0 %all-to-all-start = ((s32[64,16,4]{1,2,0:T(4,128)}), s32[64,16,4]{1,2,0:T(4,128)S(1)}, u32[]{:S(2)}, u32[]{:S(2)}) async-start(s32[64,16,4]{1,2,0:T(4,128)} %broadcast_in_dim.31), calls=%async_computation | async-start | bytes 262144 | tf_op jit(solution)/shard_map/all_to_all | solution.py:24
  49.5 8.7 %all-to-all-done = s32[64,16,4]{1,2,0:T(4,128)S(1)} async-done(((s32[64,16,4]{1,2,0:T(4,128)}), s32[64,16,4]{1,2,0:T(4,128)S(1)}, u32[]{:S(2)}, u32[]{:S(2)}) %all-to-all-start) | async-done | bytes 16416 | tf_op jit(solution)/shard_map/all_to_all | solution.py:24
  58.4 5.5 %all_to_all.30 = s32[2,1,4096]{2,1,0:T(1,128)S(1)} all-to-all(s32[2,1,4096]{2,1,0:T(1,128)S(1)} %reshape.307), channel_id=1, replica_groups=mesh['ep_0'=4,'ep_1'=4,'ep_2'=4,'tp'=2] {'tp'}, dimensions={0} | all-to-all | bytes 65536 | tf_op jit(solution)/shard_map/all_to_all | solution.py:24
  64.0 0.7 broadcast_in_dim.34
  64.6 4.7 %all-to-all-start.2 = ((f32[64,16,4]{1,2,0:T(4,128)}), f32[64,16,4]{1,2,0:T(4,128)S(1)}, u32[]{:S(2)}, u32[]{:S(2)}) async-start(f32[64,16,4]{1,2,0:T(4,128)} %broadcast_in_dim.34), calls=%async_computation.2 | async-start | bytes 262144 | tf_op jit(solution)/shard_map/all_to_all | solution.py:24
  69.9 0.8 reduce.4
  70.8 1.0 copy.142
  73.0 1.3 copy-done.3
  74.3 1.6 fusion
  76.3 1.8 all-to-all-done.2
  78.3 5.6 %all_to_all.31 = f32[2,1,4096]{2,1,0:T(1,128)S(1)} all-to-all(f32[2,1,4096]{2,1,0:T(1,128)S(1)} %reshape.309), channel_id=1, replica_groups=mesh['ep_0'=4,'ep_1'=4,'ep_2'=4,'tp'=2] {'tp'}, dimensions={0} | all-to-all | bytes 65536 | tf_op jit(solution)/shard_map/all_to_all | solution.py:24
  84.4 0.7 reduce.5
  85.2 1.0 copy.149
  87.0 2.9 %fusion.2 = f32[128,64,3]{0,1,2:T(8,128)S(1)} fusion(f32[128,64]{0,1:T(8,128)S(1)} %divide_multiply_fusion, s32[128,64,64]{0,2,1:T(8,128)S(1)} %fusion.4, s32[128,64,64]{0,2,1:T(8,128)} %copy-done.3), kind=kLoop, calls=%fused_computation.6 | loop fusion | flops 7839744 | bytes 4325376 | tf_op jit(solution)/shard_map/vmap()/reduce_sum | solution.py:96
  90.3 17.0 %all-gather.2.cloned.1.call-done = bf16[2048,1024]{1,0:T(8,128)(2,1)} async-done(((bf16[16,1024]{1,0:T(8,128)(2,1)}), bf16[2048,1024]{1,0:T(8,128)(2,1)}) %all-gather.2.cloned.1.call-update) | async-done | bytes 4194320 | tf_op jit(solution)/shard_map/all_gather | solution.py:246
  107.3 5.5 %gather_fusion = bf16[384,1024]{1,0:T(8,128)(2,1)S(1)} fusion(bf16[2048,1024]{1,0:T(8,128)(2,1)} %all-gather.2.cloned.1.call-done, s32[1024]{0:T(1024)S(1)} %pad_clamp_fusion), kind=kCustom, calls=%fused_computation | custom fusion | bytes 1574400 | tf_op jit(solution)/shard_map/gather | solution.py:257
  113.8 3.2 %fusion.5 = f32[128,1,3,1024]{3,0,2,1:T(8,128)} fusion(f32[128,3]{0,1:T(4,128)S(1)} %bitcast.128, bf16[128,3,1024]{2,1,0:T(4,128)(2,1)S(1)} %reshape.270, bf16[1,256,1024]{2,1,0:T(8,128)(2,1)S(1)} %copy-done.20, bf16[1,1024,256]{2,1,0:T(8,128)(2,1)} %param.50, f32[128,1,3,256]{3,0,2,1:T(8,128)S(1)} %convolution_bitcast_fusion.1), kind=kOutput, calls=%fused_computation.16 | convolution fusion | flops 404422656 | bytes 3802624 | tf_op jit(solution)/shard_map/necf,efd->necd/dot_general | solution.py:168
  117.0 2.5 %copy.153 = f32[128,1,3,1024]{3,2,0,1:T(4,128)S(1)} copy(f32[128,1,3,1024]{3,0,2,1:T(8,128)} %fusion.5) | data formatting | bytes 3145728 | tf_op jit(solution)/shard_map/mul | solution.py:258
  119.5 1.7 reshape.289
  121.2 3.5 %fusion.84 = f32[1,2048]{1,0:T(1,128)S(1)} fusion(bf16[2048,1024]{1,0:T(8,128)(2,1)} %all-gather.2.cloned.1.call-done, bf16[1024,1]{0,1:T(2,128)(2,1)S(1)} %reshape.301), kind=kOutput, calls=%fused_computation.149 | convolution fusion | flops 4194304 | bytes 4204544 | tf_op jit(solution)/shard_map/dot_general | solution.py:262
  124.8 1.4 fusion.85
  126.2 8.1 %convolution_multiply_fusion = f32[2048,1024]{1,0:T(8,128)} fusion(bf16[64,1024]{1,0:T(8,128)(2,1)S(1)} %copy-done.9, f32[2048]{0:T(1024)S(1)} %add_divide_fusion, bf16[2048,1024]{1,0:T(8,128)(2,1)} %all-gather.2.cloned.1.call-done, bf16[1024,64]{0,1:T(8,128)(2,1)S(1)} %copy-done.10, f32[2048,64]{0,1:T(8,128)S(1)} %fusion.85), kind=kOutput, calls=%fused_computation.8 | convolution fusion | flops 539754496 | bytes 13377536 | tf_op jit(solution)/shard_map/dot_general | solution.py:179
  134.3 10.2 %scatter_fusion = f32[2048,1024]{1,0:T(8,128)} fusion(f32[2048,1024]{1,0:T(8,128)} %convolution_multiply_fusion, s32[384]{0:T(512)S(1)} %fusion.67, f32[384,1024]{1,0:T(8,128)S(1)} %copy-done.4), kind=kCustom, calls=%fused_computation.1 | custom fusion | flops 393216 | bytes 4720128 | tf_op jit(solution)/shard_map/scatter-add | solution.py:260
  144.5 4.0 %convert_element_type.158 = bf16[2048,1024]{1,0:T(8,128)(2,1)S(1)} convert(f32[2048,1024]{1,0:T(8,128)} %scatter_fusion) | non-fusion elementwise | flops 2097152 | bytes 12582912 | tf_op jit(solution)/shard_map/convert_element_type | solution.py:269
  149.1 8.1 %all_to_all.32 = bf16[2,64,16,1024]{3,2,1,0:T(8,128)(2,1)} all-to-all(bf16[2,64,16,1024]{3,2,1,0:T(8,128)(2,1)S(1)} %bitcast.117), channel_id=1, replica_groups=mesh['ep_0'=4,'ep_1'=4,'ep_2'=4,'tp'=2] {'tp'}, dimensions={0} | all-to-all | bytes 8388608 | tf_op jit(solution)/shard_map/all_to_all | solution.py:50
  157.2 5.4 %reduce_sum.120 = bf16[64,16,1024]{2,1,0:T(8,128)(2,1)} reduce(bf16[2,64,16,1024]{3,2,1,0:T(8,128)(2,1)} %all_to_all.32, bf16[]{:T(256)} %constant.89.clone.1), dimensions={0}, to_apply=%region_12.13 | reduce | flops 1048576 | bytes 6291458 | tf_op jit(solution)/shard_map/reduce_sum | solution.py:51
  162.5 6.8 %all-to-all-start.5 = ((bf16[64,16,1024]{2,1,0:T(8,128)(2,1)}), bf16[64,16,1024]{2,1,0:T(8,128)(2,1)}, u32[]{:S(2)}, u32[]{:S(2)}) async-start(bf16[64,16,1024]{2,1,0:T(8,128)(2,1)} %reduce_sum.120), calls=%async_computation.5 | async-start | bytes 4194304 | tf_op jit(solution)/shard_map/all_to_all | solution.py:58
  169.3 1.5 fusion.86
  170.8 27.3 %all-to-all-done.5 = bf16[64,16,1024]{2,1,0:T(8,128)(2,1)} async-done(((bf16[64,16,1024]{2,1,0:T(8,128)(2,1)}), bf16[64,16,1024]{2,1,0:T(8,128)(2,1)}, u32[]{:S(2)}, u32[]{:S(2)}) %all-to-all-start.5) | async-done | bytes 2097184 | tf_op jit(solution)/shard_map/all_to_all | solution.py:58
  198.1 1.9 convert_reduce_fusion
  200.1 1.8 multiply_reduce_fusion
  201.9 0.7 fusion.53
  (113 shorter events, 9.5 us)
Async XLA Ops:
  7.2 28.2 %copy-start = (bf16[1024,1024]{1,0:T(8,128)(2,1)S(1)}, bf16[1024,1024]{1,0:T(8,128)(2,1)}, u32[]{:S(2)}) copy-start(bf16[1024,1024]{1,0:T(8,128)(2,1)} %param.44) | copy-start | bytes 6291460
  7.2 13.0 %copy-start.8 = (bf16[16,1024]{1,0:T(8,128)(2,1)S(1)}, bf16[16,1024]{1,0:T(8,128)(2,1)}, u32[]{:S(2)}) copy-start(bf16[16,1024]{1,0:T(8,128)(2,1)} %param.30) | copy-start | bytes 98308
  7.2 14.3 %copy-start.21 = (bf16[256]{0:T(256)(128)(2,1)S(1)}, bf16[256]{0:T(256)(128)(2,1)}, u32[]{:S(2)}) copy-start(bf16[256]{0:T(256)(128)(2,1)} %param.40) | copy-start | bytes 1540
  7.2 100.1 %all-gather.2.cloned.1.call-start = ((), (), s32[]{:S(2)}) async-start(), calls=%async_computation.6 | async-start | bytes 4227072 | tf_op jit(solution)/shard_map/all_gather | solution.py:246
  21.8 5.9 %copy-start.12 = (bf16[16,256]{1,0:T(8,128)(2,1)}, bf16[16,256]{1,0:T(8,128)(2,1)S(1)}, u32[]{:S(2)}) copy-start(bf16[16,256]{1,0:T(8,128)(2,1)S(1)} %get-tuple-element.7) | copy-start | bytes 24580
  30.2 4.8 %copy-start.5 = (bf16[256,1024]{0,1:T(8,128)(2,1)S(1)}, bf16[256,1024]{0,1:T(8,128)(2,1)}, u32[]{:S(2)}) copy-start(bf16[256,1024]{0,1:T(8,128)(2,1)} %copy.138) | copy-start | bytes 1572868
  30.2 5.7 %copy-start.15 = (bf16[1024]{0:T(1024)(128)(2,1)S(1)}, bf16[1024]{0:T(1024)(128)(2,1)}, u32[]{:S(2)}) copy-start(bf16[1024]{0:T(1024)(128)(2,1)} %param.45) | copy-start | bytes 6148
  30.2 5.9 %copy-start.16 = (bf16[1024]{0:T(1024)(128)(2,1)S(1)}, bf16[1024]{0:T(1024)(128)(2,1)}, u32[]{:S(2)}) copy-start(bf16[1024]{0:T(1024)(128)(2,1)} %param.46) | copy-start | bytes 6148
  30.2 6.6 %copy-start.13 = (s32[16,4]{0,1:T(4,128)S(1)}, s32[16,4]{0,1:T(4,128)}, u32[]{:S(2)}) copy-start(s32[16,4]{0,1:T(4,128)} %param.47) | copy-start | bytes 772
  30.2 19.3 %copy-start.17 = (bf16[1024]{0:T(1024)(128)(2,1)S(1)}, bf16[1024]{0:T(1024)(128)(2,1)}, u32[]{:S(2)}) copy-start(bf16[1024]{0:T(1024)(128)(2,1)} %param.55) | copy-start | bytes 6148
  34.9 29.0 %copy-start.14 = (f32[16,4]{0,1:T(4,128)S(1)}, f32[16,4]{0,1:T(4,128)}, u32[]{:S(2)}) copy-start(f32[16,4]{0,1:T(4,128)} %param.48) | copy-start | bytes 772
  37.5 20.7 %all-to-all-start = ((s32[64,16,4]{1,2,0:T(4,128)}), s32[64,16,4]{1,2,0:T(4,128)S(1)}, u32[]{:S(2)}, u32[]{:S(2)}) async-start(s32[64,16,4]{1,2,0:T(4,128)} %broadcast_in_dim.31), calls=%async_computation | async-start | bytes 262144 | tf_op jit(solution)/shard_map/all_to_all | solution.py:24
  64.6 13.5 %all-to-all-start.2 = ((f32[64,16,4]{1,2,0:T(4,128)}), f32[64,16,4]{1,2,0:T(4,128)S(1)}, u32[]{:S(2)}, u32[]{:S(2)}) async-start(f32[64,16,4]{1,2,0:T(4,128)} %broadcast_in_dim.34), calls=%async_computation.2 | async-start | bytes 262144 | tf_op jit(solution)/shard_map/all_to_all | solution.py:24
  73.0 1.4 copy-start.3
  90.3 23.0 %copy-start.19 = (bf16[1,1024,256]{2,1,0:T(8,128)(2,1)S(1)}, bf16[1,1024,256]{2,1,0:T(8,128)(2,1)}, u32[]{:S(2)}) copy-start(bf16[1,1024,256]{2,1,0:T(8,128)(2,1)} %param.49) | copy-start | bytes 1572868
  90.3 23.6 %copy-start.20 = (bf16[1,256,1024]{2,1,0:T(8,128)(2,1)S(1)}, bf16[1,256,1024]{2,1,0:T(8,128)(2,1)}, u32[]{:S(2)}) copy-start(bf16[1,256,1024]{2,1,0:T(8,128)(2,1)} %param.51) | copy-start | bytes 1572868
  119.5 5.3 %copy-start.11 = (bf16[1024,64]{0,1:T(8,128)(2,1)S(1)}, bf16[1024,64]{0,1:T(8,128)(2,1)}, u32[]{:S(2)}) copy-start(bf16[1024,64]{0,1:T(8,128)(2,1)} %param.56) | copy-start | bytes 393220
  121.2 3.6 %copy-start.2 = (bf16[2048,1024]{1,0:T(8,128)(2,1)S(1)}, bf16[2048,1024]{1,0:T(8,128)(2,1)}, u32[]{:S(2)}) copy-start(bf16[2048,1024]{1,0:T(8,128)(2,1)} %all-gather.2.cloned.1.call-done) | copy-start | bytes 12582916
  124.8 1.4 copy-start.9
  124.8 1.4 copy-start.10
  126.2 8.1 %copy-start.4 = (f32[384,1024]{1,0:T(8,128)S(1)}, f32[384,1024]{1,0:T(8,128)}, u32[]{:S(2)}) copy-start(f32[384,1024]{1,0:T(8,128)} %reshape.289) | copy-start | bytes 4718596
  157.2 12.2 %copy-start.18 = (bf16[1024]{0:T(1024)(128)(2,1)S(1)}, bf16[1024]{0:T(1024)(128)(2,1)}, u32[]{:S(2)}) copy-start(bf16[1024]{0:T(1024)(128)(2,1)} %param.59) | copy-start | bytes 6148
  157.2 12.2 %copy-start.7 = (bf16[16,1024]{1,0:T(8,128)(2,1)S(1)}, bf16[16,1024]{1,0:T(8,128)(2,1)}, u32[]{:S(2)}) copy-start(bf16[16,1024]{1,0:T(8,128)(2,1)} %fusion.52) | copy-start | bytes 98308
  157.2 45.4 %copy-start.1 = (bf16[1024,1024]{1,0:T(8,128)(2,1)S(1)}, bf16[1024,1024]{1,0:T(8,128)(2,1)}, u32[]{:S(2)}) copy-start(bf16[1024,1024]{1,0:T(8,128)(2,1)} %param.44) | copy-start | bytes 6291460
  162.5 37.5 %copy-start.6 = (bf16[512,1024]{1,0:T(8,128)(2,1)S(1)}, bf16[512,1024]{1,0:T(8,128)(2,1)}, u32[]{:S(2)}) copy-start(bf16[512,1024]{1,0:T(8,128)(2,1)} %param.54) | copy-start | bytes 3145732
  162.5 35.6 %all-to-all-start.5 = ((bf16[64,16,1024]{2,1,0:T(8,128)(2,1)}), bf16[64,16,1024]{2,1,0:T(8,128)(2,1)}, u32[]{:S(2)}, u32[]{:S(2)}) async-start(bf16[64,16,1024]{2,1,0:T(8,128)(2,1)} %reduce_sum.120), calls=%async_computation.5 | async-start | bytes 4194304 | tf_op jit(solution)/shard_map/all_to_all | solution.py:58
Sparse Core Ops, SparseCore 0:
  37.0 70.2 all-gather.1
where the time goes:
time: 211 us; the launch traced here: 209 us
  waiting for transfers between devices  54.8 us (26%)
  matrix products  40.2 us (19%)
  other arithmetic  34.5 us (16%)
  starting transfers between devices  23.4 us (11%)
  local copies, waits for them, and re-layouts  22.8 us (11%)
  blocking collectives  19.2 us (9%)
  between operations  14.6 us (7%)
    all_to_all x1, waiting for transfers between devices, sum_in_two_steps(): lax.all_to_all(nearer.astype(jnp.bfloat16), far, split_axis=0, concat_axi...  27.3 us
    all_gather x1, waiting for transfers between devices, shards(): every_rows = lax.all_gather(moe_in, EP_TP, axis=0, tiled=True)  17 us
    all_to_all x2, starting transfers between devices, from_everyone(): lax.all_to_all(jnp.broadcast_to(shard[None], (devices, *shard.shape)), ax...  16.6 us
    all_to_all x2, blocking collectives, from_everyone(): lax.all_to_all(jnp.broadcast_to(shard[None], (devices, *shard.shape)), ax...  11.1 us
    all_to_all x2, waiting for transfers between devices, from_everyone(): lax.all_to_all(jnp.broadcast_to(shard[None], (devices, *shard.shape)), ax...  10.6 us
    scatter-add x1, other arithmetic, shards(): jnp.zeros(every_rows.shape, f32).at[where_rows.reshape(-1)]  10.2 us
    all_to_all x1, blocking collectives, sum_at_owner(): lax.all_to_all(in_blocks(shard, dim, devices), axis, 0, 0, tiled=True)  8.09 us
    dot_general x1, matrix products, dense_partial(): return jnp.dot(act, w_down, preferred_element_type=jnp.float32)  8.07 us
  transfers between devices with their start and end apart: 4, of which 4 were waited for; matrix products, arithmetic and copies ran while one was open for 7% of the time, Pallas kernels for 0%

commit v1 on v0

v1 whole, which is shorter than its diff:
```python
import math

import jax
import jax.numpy as jnp
from jax import lax
from jax.experimental import pallas as pl
from jax.experimental.pallas import tpu as pltpu
from jax.sharding import PartitionSpec as P

f32 = jnp.float32
bf16 = jnp.bfloat16
EPS = 1e-6
NT = (((1,), (1,)), ((), ()))
NN = (((1,), (0,)), ((), ()))
TN = (((0,), (0,)), ((), ()))
MESH = pl.DeviceIdType.MESH

S, H, NOPE, ROPE, L, C, D = 16, 16, 64, 32, 1024, 256, 1024
SCALE = (NOPE + ROPE) ** -0.5
CHIPS, PLANE = 64, 16
SLOTS, QB = 4, 4
PIECE = SLOTS * QB


def dot(a, b, dims=NN):
    return lax.dot_general(a, b, dims, preferred_element_type=f32)


def iota(shape, dim):
    return lax.broadcasted_iota(jnp.int32, shape, dim)


def row_of(ref):
    blocks = ref[...].astype(f32)
    return jnp.concatenate([blocks[r : r + 1, :] for r in range(blocks.shape[0])], axis=1)


def rms(value, gain):
    inverse = lax.rsqrt(jnp.mean(value * value, axis=-1, keepdims=True) + EPS)
    return value * inverse * gain


def silu(v):
    return v / (1.0 + jnp.exp(-v))


def rope_tables(len_ref):
    half = ROPE // 2
    lane = iota((S, 128), 1) % half
    row = iota((S, 128), 0)
    pos = jnp.zeros((S, 128), jnp.int32)
    for s in range(S):
        pos = jnp.where(row == s, len_ref[s], pos)
    freq = jnp.exp(lane.astype(f32) * (-math.log(10000.0) / half))
    angle = pos.astype(f32) * freq
    return jnp.cos(angle), jnp.sin(angle)


def rotate128(value, cosine, sine):
    half = ROPE // 2
    first = (iota(value.shape, 1) % ROPE) < half
    other = jnp.where(first, -pltpu.roll(value, 128 - half, 1), pltpu.roll(value, half, 1))
    return value * cosine + other * sine


def halves(value):
    high = value.astype(bf16)
    return high, (value - high.astype(f32)).astype(bf16)


def route_tables(routes, scores, pick, weigh):
    ids = routes[...].astype(bf16)
    spread = (iota((S, QB * S), 1) % S == iota((S, QB * S), 0)).astype(bf16)
    named = dot(ids, spread)
    expert = iota((CHIPS, QB * S), 0).astype(f32)
    count = jnp.zeros((CHIPS, QB * S), f32)
    for k in range(4):
        count += jnp.where(named[k : k + 1, :] == expert, 1.0, 0.0)
    r, c = iota((QB * S, QB * S), 0), iota((QB * S, QB * S), 1)
    before = ((r < S) & (r < c % S)).astype(bf16)
    rank = dot(count.astype(bf16), before)
    at = jnp.where(count > 0.5, rank, -1.0)
    shape = (CHIPS, PIECE, QB * S)
    i, n = iota(shape, 1), iota(shape, 2)
    here = (at[:, None, :] == (i % SLOTS).astype(f32)) & (i // SLOTS == n // S)
    pick[...] = jnp.where(here, 1.0, 0.0).reshape(CHIPS * PIECE, QB * S).astype(bf16)

    norm = scores[...]
    norm = norm / jnp.sum(norm, axis=0, keepdims=True) * 2.5
    high, low = halves(norm)
    select = (iota((QB * S, S), 0) % S == iota((QB * S, S), 1)).astype(bf16)
    named_t, high_t, low_t = dot(select, ids, NT), dot(select, high, NT), dot(select, low, NT)
    expert_t = iota((QB * S, CHIPS), 1).astype(f32)
    count_t = jnp.zeros((QB * S, CHIPS), f32)
    w_high, w_low = count_t, count_t
    for k in range(4):
        hit = named_t[:, k : k + 1] == expert_t
        count_t += jnp.where(hit, 1.0, 0.0)
        w_high += jnp.where(hit, high_t[:, k : k + 1], 0.0)
        w_low += jnp.where(hit, low_t[:, k : k + 1], 0.0)
    before_t = ((c < S) & (c < r % S)).astype(bf16)
    rank_t = dot(before_t, count_t.astype(bf16))
    widen = (iota((CHIPS, CHIPS * PIECE), 1) // PIECE == iota((CHIPS, CHIPS * PIECE), 0)).astype(bf16)
    shape = (QB * S, CHIPS * PIECE)
    m = iota(shape, 1)
    here = (dot(rank_t.astype(bf16), widen) == (m % SLOTS).astype(f32)) & (
        (m // SLOTS) % QB == iota(shape, 0) // S
    )
    weigh[0 : QB * S, :] = jnp.where(here, dot(w_high.astype(bf16), widen), 0.0).astype(bf16)
    weigh[QB * S : 2 * QB * S, :] = jnp.where(here, dot(w_low.astype(bf16), widen), 0.0).astype(bf16)


def kernel(
    len_ref, tok_h, lat_h, rope_h, ag, wdq_h, qg, wqn_h, wqr_h, wdkv_h, kvg, wkr_h, wuk_h, wuv_h, wo_h, pg, mg,
    routes, scores, eg_h, eu_h, ed_h, sg_h, su_h, sd_h, dvec, dg_h, du_h, dd_h, og,
    out_o, lat_o,
    tok, lat, rope, wdq, wqn, wqr, wdkv, wkr, wuk, wuv, wo, ql, qr, own_s, mixed, nlat,
    eg, eu, ed, sg, su, sd, dg, du, dd, pick, weigh,
    moe, send, recv, back, home, rows, parts, sums,
    sems, lsem, esem, dsem, zsem_s, zsem_r, fsem_s, fsem_r, asem_s, asem_r, bsem_s, bsem_r, gsem_s, gsem_r, psem_s, psem_r,
):
    ep = lax.axis_index("ep")
    tp = lax.axis_index("tp")
    z, y, x = ep // 16, (ep // 4) % 4, ep % 4
    plane = ep % 16

    def remote(src, dst, s_sem, r_sem, chip, core):
        return pltpu.make_async_remote_copy(
            src_ref=src, dst_ref=dst, send_sem=s_sem, recv_sem=r_sem, device_id=(chip, core), device_id_type=MESH
        )

    early = [(tok_h, tok), (wdq_h, wdq), (wdkv_h, wdkv), (wkr_h, wkr), (wqn_h, wqn), (wqr_h, wqr), (wuk_h, wuk)]
    late = [(wuv_h, wuv), (wo_h, wo), (eg_h, eg.at[0:1]), (eu_h, eu.at[0:1]), (ed_h, ed.at[0:1]),
            (sg_h, sg), (su_h, su), (sd_h, sd), (dg_h, dg.at[0]), (du_h, du.at[0]), (dd_h, dd.at[0])]
    early = [pltpu.make_async_copy(a, b, sems.at[i]) for i, (a, b) in enumerate(early)]
    late = [pltpu.make_async_copy(a, b, sems.at[7 + i]) for i, (a, b) in enumerate(late)]

    def lat_cp(g):
        return (
            pltpu.make_async_copy(lat_h.at[pl.ds(4 * g, 4)], lat.at[pl.ds(4 * g, 4)], lsem.at[g, 0]),
            pltpu.make_async_copy(rope_h.at[pl.ds(4 * g, 4)], rope.at[pl.ds(4 * g, 4)], lsem.at[g, 1]),
        )

    for c in early:
        c.start()
    for g in range(4):
        for c in lat_cp(g):
            c.start()
    for c in late:
        c.start()

    barrier = pltpu.get_barrier_semaphore()

    def chip_of(k):
        kz, ky, kx = k // 16, (k // 4) % 4, k % 4
        return ((z + kz) % 4) * 16 + ((y + ky) % 4) * 4 + (x + kx) % 4

    def greet(k, _):
        pl.semaphore_signal(barrier, inc=1, device_id=(chip_of(k), tp), device_id_type=MESH)
        return 0

    lax.fori_loop(1, CHIPS, greet, 0)
    pl.semaphore_signal(barrier, inc=1, device_id=(ep, 1 - tp), device_id_type=MESH)

    route_tables(routes, scores, pick, weigh)

    cosine, sine = rope_tables(len_ref)
    early[0].wait()
    tokens = tok[...].astype(f32)
    normed = rms(tokens, row_of(ag)).astype(bf16)
    early[1].wait()
    qn = rms(dot(normed, wdq[...]), row_of(qg)).astype(bf16)
    early[2].wait()
    nl = rms(dot(normed, wdkv[...]), row_of(kvg)).astype(bf16)
    nlat[...] = nl.astype(f32)
    lat_o[...] = nl
    early[3].wait()
    kr = dot(normed, jnp.concatenate([wkr[...]] * 4, axis=0), NT)
    kr = rotate128(kr, cosine, sine).astype(bf16)
    early[4].wait()
    qnope = dot(qn, wqn[...]).astype(bf16).astype(f32)
    head = iota((H, D), 1) // NOPE == iota((H, D), 0)
    qm = jnp.where(head[None], qnope[:, None, :], 0.0).reshape(S * H, D).astype(bf16)
    early[5].wait()
    qraw = dot(qn, wqr[...])
    qrot = jnp.concatenate(
        [rotate128(qraw[:, 128 * i : 128 * i + 128], cosine, sine) for i in range(4)], axis=1
    )
    qrot = qrot.astype(bf16).astype(f32)
    headr = iota((H, H * ROPE), 1) // ROPE == iota((H, H * ROPE), 0)
    qrm = jnp.where(headr[None], qrot[:, None, :], 0.0).reshape(S * H, H * ROPE).astype(bf16)
    fold = (iota((H * ROPE, 128), 0) % ROPE == iota((H * ROPE, 128), 1)).astype(bf16)
    qrf = dot(qrm, fold)
    qr[...] = qrf.astype(bf16)
    early[6].wait()
    qlat = dot(qm, wuk[...], NT).astype(bf16)
    ql[...] = qlat
    own = jnp.sum(qlat.astype(f32).reshape(S, H, C) * nl.astype(f32)[:, None, :], axis=-1, keepdims=True)
    own += jnp.sum(qrf.reshape(S, H, 128) * kr.astype(f32)[:, None, :], axis=-1, keepdims=True)
    own_s[...] = own.reshape(S * H, 1) * SCALE

    pl.semaphore_wait(barrier, CHIPS)
    up_chip = ((z + 1) % 4) * 16 + plane
    down_chip = ((z + 3) % 4) * 16 + plane
    to_core = [
        remote(eg_h, eg.at[1:2], esem.at[0, 0], esem.at[1, 0], ep, 1 - tp),
        remote(eu_h, eu.at[1:2], esem.at[0, 1], esem.at[1, 1], ep, 1 - tp),
        remote(ed_h, ed.at[1:2], esem.at[0, 2], esem.at[1, 2], ep, 1 - tp),
        remote(dg_h, dg.at[4], esem.at[0, 3], esem.at[1, 3], ep, 1 - tp),
        remote(du_h, du.at[4], esem.at[0, 4], esem.at[1, 4], ep, 1 - tp),
        remote(dd_h, dd.at[4], esem.at[0, 5], esem.at[1, 5], ep, 1 - tp),
    ]
    to_chips = []
    for i, (h, buf) in enumerate([(dg_h, dg), (du_h, du), (dd_h, dd)]):
        to_chips.append(remote(h, buf.at[1], zsem_s.at[0, i], zsem_r.at[0, i], up_chip, tp))
        to_chips.append(remote(h, buf.at[3], zsem_s.at[1, i], zsem_r.at[1, i], down_chip, tp))
    for c in to_chips + to_core:
        c.start()

    lane = iota((H, L), 1)

    def group(g, _):
        for c in lat_cp(g):
            c.wait()
        base = pl.multiple_of(g * 4 * H, 4 * H)
        rows4 = pl.ds(base, 4 * H)
        sc = jnp.concatenate(
            [
                dot(ql[pl.ds(base + i * H, H)], lat[g * 4 + i], NT)
                + dot(qr[pl.ds(base + i * H, H), :][:, :ROPE], rope[g * 4 + i])
                for i in range(4)
            ],
            axis=0,
        )
        sc = sc * SCALE
        valid = jnp.concatenate([lane < len_ref[g * 4 + i] for i in range(4)], axis=0)
        ow = own_s[rows4]
        top = jnp.maximum(jnp.max(jnp.where(valid, sc, -1e30), axis=-1, keepdims=True), ow)
        w = jnp.where(valid, jnp.exp(sc - top), 0.0)
        ow = jnp.exp(ow - top)
        inv = 1.0 / (jnp.sum(w, axis=-1, keepdims=True) + ow)
        pb = (w * inv).astype(bf16)
        ob = (ow * inv).astype(bf16).astype(f32)
        for i in range(4):
            m = dot(pb[i * H : i * H + H], lat[g * 4 + i]) + ob[i * H : i * H + H] * nlat[pl.ds(g * 4 + i, 1)]
            mixed[pl.ds(base + i * H, H)] = m.astype(bf16)
        return 0

    lax.fori_loop(0, 4, group, 0)
    late[0].wait()
    full = dot(mixed[...], wuv[...]).reshape(S, H, D)
    ho = jnp.sum(jnp.where(head[None], full, 0.0), axis=1).astype(bf16)
    late[1].wait()
    first = (tokens + rms(dot(ho, wo[...]), row_of(pg))).astype(bf16)
    moe_in = rms(first.astype(f32), row_of(mg)).astype(bf16)
    moe[...] = moe_in

    blocks = jnp.concatenate([moe_in[:, 256 * q : 256 * q + 256] for q in range(QB)], axis=0)
    send[...] = dot(pick[...], blocks).astype(bf16).reshape(CHIPS, PIECE, 256)
    recv[ep] = send[ep]
    rows[plane] = moe_in

    def dispatch(k, _):
        chip = chip_of(k)
        remote(send.at[chip], recv.at[ep], asem_s, asem_r.at[k // 16], chip, tp).start()
        return 0

    def gather(k, _):
        chip = chip_of(k)
        remote(moe, rows.at[plane], gsem_s, gsem_r, chip, tp).start()
        return 0

    lax.fori_loop(1, CHIPS, dispatch, 0)
    lax.fori_loop(1, PLANE, gather, 0)

    for i, buf in enumerate([dg, du, dd]):
        remote(buf.at[1], buf.at[1], zsem_s.at[0, i], zsem_r.at[0, i], up_chip, tp).wait_recv()
        remote(buf.at[3], buf.at[3], zsem_s.at[1, i], zsem_r.at[1, i], down_chip, tp).wait_recv()
    onward = jnp.where(tp == 0, 1, 3)
    next_chip = jnp.where(tp == 0, up_chip, down_chip)
    onwards, crossing = [], []
    for i, buf in enumerate([dg, du, dd]):
        onwards.append(remote(buf.at[onward], buf.at[2], fsem_s.at[0, i], fsem_r.at[0, i], next_chip, tp))
    for i, buf in enumerate([dg, du, dd]):
        crossing.append(remote(buf.at[1], buf.at[5], fsem_s.at[1, i], fsem_r.at[1, i], ep, 1 - tp))
        crossing.append(remote(buf.at[3], buf.at[7], fsem_s.at[2, i], fsem_r.at[2, i], ep, 1 - tp))
    for c in onwards + crossing:
        c.start()

    for c in late[5:8]:
        c.wait()
    shared_act = (silu(dot(moe_in, sg[...])) * dot(moe_in, su[...])).astype(bf16)
    mixture = dot(shared_act, sd[...])

    for c in late[2:5]:
        c.wait()
    for c in to_core[0:3]:
        c.wait_recv()
    m, n = iota((256, 256), 0), iota((256, 256), 1)
    sort = ((m // 64 == (n // SLOTS) % QB) & ((m % 64) // SLOTS == n // PIECE) & (m % SLOTS == n % SLOTS))
    sort = jnp.where(sort, 1.0, 0.0).astype(bf16)
    for i in range(4):
        g = (z + 4 - i) % 4
        lo = pl.multiple_of(g * PLANE, PLANE)
        if i == 0:
            pltpu.make_async_copy(recv.at[0:15], recv.at[0:15], asem_r.at[0]).wait()
        else:
            pltpu.make_async_copy(recv.at[0:16], recv.at[0:16], asem_r.at[i]).wait()
        got = dot(sort, recv[pl.ds(lo, PLANE)].reshape(PLANE * PIECE, 256)).astype(bf16)
        rows_in = jnp.concatenate([got[64 * q : 64 * q + 64] for q in range(QB)], axis=1)
        total = jnp.zeros((64, D), f32)
        for part in range(2):
            act = (silu(dot(rows_in, eg[part])) * dot(rows_in, eu[part])).astype(bf16)
            total += dot(act, ed[part]).astype(bf16).astype(f32)
        total = total.astype(bf16)
        total = jnp.concatenate([total[:, 256 * q : 256 * q + 256] for q in range(QB)], axis=0)
        back[pl.ds(lo, PLANE)] = dot(sort, total, TN).astype(bf16).reshape(PLANE, PIECE, 256)
        if i == 0:
            home[ep] = back[ep]

        def give(k, _):
            chip = chip_of(((4 - i) % 4) * 16 + k)
            remote(back.at[chip], home.at[ep], bsem_s, bsem_r, chip, tp).start()
            return 0

        lax.fori_loop(1 if i == 0 else 0, PLANE, give, 0)

    for c in onwards:
        c.wait_recv()
    last = [
        remote(buf.at[2], buf.at[6], fsem_s.at[3, i], fsem_r.at[3, i], ep, 1 - tp) for i, buf in enumerate([dg, du, dd])
    ]
    for c in last:
        c.start()
    for c in late[8:11]:
        c.wait()
    for c in to_core[3:6] + crossing + last:
        c.wait_recv()
    pltpu.make_async_copy(rows.at[0:15], rows.at[0:15], gsem_r).wait()
    all_rows = rows[...].reshape(PLANE * S, D)
    gate_h = dot(all_rows, dg[...].reshape(512, D), NT)
    up_h = dot(all_rows, du[...].reshape(512, D), NT)
    act = (silu(gate_h) * up_h).astype(bf16)
    parts[...] = dot(act, dd[...].reshape(512, D)).astype(bf16).reshape(PLANE, S, D)
    sums[plane] = parts[plane]

    def share(k, _):
        chip = chip_of(k)
        remote(parts.at[chip % 16], sums.at[plane], psem_s, psem_r, chip, tp).start()
        return 0

    lax.fori_loop(1, PLANE, share, 0)

    gate = jnp.sum(moe_in.astype(f32) * row_of(dvec), axis=-1, keepdims=True)
    gate = 1.0 / (1.0 + jnp.exp(-gate))

    pltpu.make_async_copy(home.at[0:63], home.at[0:63], bsem_r).wait()
    routed = dot(weigh[...], home[...].reshape(CHIPS * PIECE, 256))
    routed = routed[0:64] + routed[64:128]
    mixture += jnp.concatenate([routed[S * q : S * q + S] for q in range(QB)], axis=1)

    pltpu.make_async_copy(sums.at[0:15], sums.at[0:15], psem_r).wait()
    dense = jnp.zeros((S, D), f32)
    for p in range(PLANE):
        dense += sums[p].astype(f32)
    mixture += gate * dense
    out_o[...] = (first.astype(f32) + rms(mixture, row_of(og))).astype(bf16)

    for c in to_chips + to_core + onwards + crossing + last:
        c.wait_send()
    pltpu.make_async_copy(send.at[0:63], send.at[0:63], asem_s).wait()
    pltpu.make_async_copy(back.at[0:63], back.at[0:63], bsem_s).wait()
    pltpu.make_async_copy(rows.at[0:15], rows.at[0:15], gsem_s).wait()
    pltpu.make_async_copy(parts.at[0:15], parts.at[0:15], psem_s).wait()


def step(
    tokens, lengths, latent, rope, ag, wdq, qg, wqn, wqr, wdkv, kvg, wkr, wuk, wuv, wo, pg, mg,
    routes, scores, eg, eu, ed, sg, su, sd, dvec, dg, du, dd, og,
):
    anyspec = pl.BlockSpec(memory_space=pl.ANY)
    vm = pl.BlockSpec(memory_space=pltpu.VMEM)
    smem = pl.BlockSpec(memory_space=pltpu.SMEM)

    def tile(v):
        return v.reshape(v.shape[0] // 128, 128)

    operands = [
        (lengths, smem), (tokens, anyspec), (latent, anyspec), (rope, anyspec), (tile(ag), vm), (wdq, anyspec), (tile(qg), vm),
        (wqn, anyspec), (wqr, anyspec), (wdkv, anyspec), (tile(kvg), vm), (wkr.T, anyspec), (wuk, anyspec), (wuv, anyspec),
        (wo, anyspec), (tile(pg), vm), (tile(mg), vm), (routes.T, vm), (scores.T, vm), (eg, anyspec), (eu, anyspec),
        (ed, anyspec), (sg, anyspec), (su, anyspec), (sd, anyspec), (tile(dvec), vm), (dg.T, anyspec), (du.T, anyspec),
        (dd, anyspec), (tile(og), vm),
    ]

    def v(*shape, dtype=bf16):
        return pltpu.VMEM(shape, dtype)

    dma = pltpu.SemaphoreType.DMA
    scratch = [
        v(16, 1024), v(16, 1024, 256), v(16, 32, 1024), v(1024, 512), v(512, 1024), v(512, 512), v(1024, 256), v(32, 1024),
        v(256, 1024), v(256, 1024), v(1024, 1024),
        v(256, 256), v(256, 128), v(256, 1, dtype=f32), v(256, 256), v(16, 256, dtype=f32),
        v(2, 1024, 256), v(2, 1024, 256), v(2, 256, 1024), v(1024, 512), v(1024, 512), v(512, 1024),
        v(8, 64, 1024), v(8, 64, 1024), v(8, 64, 1024), v(1024, 64), v(128, 1024),
        v(16, 1024), v(64, 16, 256), v(64, 16, 256), v(64, 16, 256), v(64, 16, 256), v(16, 16, 1024), v(16, 16, 1024), v(16, 16, 1024),
        dma((18,)), dma((4, 2)), dma((2, 6)), dma((1,)), dma((2, 3)), dma((2, 3)), dma((4, 3)), dma((4, 3)),
        dma, dma((4,)), dma, dma, dma, dma, dma, dma,
    ]
    return pl.pallas_call(
        kernel,
        out_shape=[jax.ShapeDtypeStruct((S, D), bf16), jax.ShapeDtypeStruct((S, C), bf16)],
        in_specs=[s for _, s in operands],
        out_specs=[vm, vm],
        scratch_shapes=scratch,
        compiler_params=pltpu.CompilerParams(
            collective_id=0, has_side_effects=True, vmem_limit_bytes=62 * 2**20
        ),
    )(*[a for a, _ in operands])


def solution(mesh):
    both = ("ep", "tp")
    by_token, whole = P(both, None), P()
    placed = (
        by_token, P(both), P(both, None, None), P(both, None, None),
        whole, whole, whole, whole, whole, whole, whole, whole, whole, whole, whole, whole, whole,
        by_token, by_token,
        P("ep", None, "tp"), P("ep", None, "tp"), P("ep", "tp", None),
        whole, whole, whole, whole,
        P(None, both), P(None, both), P(both, None), whole,
    )
    return jax.shard_map(step, mesh=mesh, in_specs=placed, out_specs=(by_token, by_token), check_vma=False)
```

time: 211 us -> 54.5 us (0.26)
  waiting for transfers between devices: 54.8 us -> 0 us
  Pallas kernels: 0 us -> 50.9 us
  matrix products: 40.2 us -> 0 us
  other arithmetic: 34.5 us -> 0 us
  starting transfers between devices: 23.4 us -> 0 us
  local copies, waits for them, and re-layouts: 22.8 us -> 2.67 us
  blocking collectives: 19.2 us -> 0 us
  between operations: 14.6 us -> 0.65 us
    pallas_call x0 -> x1, Pallas kernels: none -> 50.9 us  [step(): pl.pallas_call(kernel, out_shape=[jax.ShapeDtypeStruct((S, D), bf16), jax...]
    dot_general x20 -> x0, matrix products: 40.2 us -> none  [the longest x1 8.07 us: dense_partial(): return jnp.dot(act, w_down, preferred_element_type=jnp.float32)]
    all_to_all x3 -> x0, waiting for transfers between devices: 37.9 us -> none  [the longest x1 27.3 us: sum_in_two_steps(): lax.all_to_all(nearer.astype(jnp.bfloat16), far, split_axis=0, concat_axi...]
    all_to_all x3 -> x0, starting transfers between devices: 23.4 us -> none  [the longest x2 16.6 us: from_everyone(): lax.all_to_all(jnp.broadcast_to(shard[None], (devices, *shard.shape)), ax...]
    all_to_all x3 -> x0, blocking collectives: 19.2 us -> none  [the longest x2 11.1 us: from_everyone(): lax.all_to_all(jnp.broadcast_to(shard[None], (devices, *shard.shape)), ax...]
    all_gather x1 -> x0, waiting for transfers between devices: 17 us -> none  [shards(): every_rows = lax.all_gather(moe_in, EP_TP, axis=0, tiled=True)]
    reduce_sum x8 -> x0, other arithmetic: 13.2 us -> none  [the longest x1 5.38 us: sum_at_owner(): return jnp.sum(tiles.astype(jnp.float32), axis=0)]
    scatter-add x1 -> x0, other arithmetic: 10.2 us -> none  [shards(): jnp.zeros(every_rows.shape, f32).at[where_rows.reshape(-1)]]
  transfers between devices with their start and end apart: 4 -> 0, of which waited for: 4 -> 0; matrix products, arithmetic and copies ran while one was open for 7% -> 0% of each run, Pallas kernels for 0% -> 0%
where the time goes in v1:
time: 54.5 us; the launch traced here: 54.3 us
  Pallas kernels  50.9 us (93%)
  local copies, waits for them, and re-layouts  2.67 us (5%)
  between operations  0.65 us (1%)
    pallas_call x1, Pallas kernels, step(): pl.pallas_call(kernel, out_shape=[jax.ShapeDtypeStruct((S, D), bf16), jax...  50.9 us
    unnamed x2, local copies, waits for them, and re-layouts  2.67 us

profile of v1, /device:TPU:1, one launch (start us, length us, event | category | flops | bytes accessed | tf_op | source)
XLA Modules:
  0.0 54.3 jit_solution(12832863052619385367)
XLA Ops:
  0.6 50.9 %shard_map.293 = (bf16[16,1024]{1,0:T(8,128)(2,1)}, bf16[16,256]{1,0:T(8,128)(2,1)}) custom-call(s32[16]{0:T(128)} %len_ref.1, bf16[16,1024]{1,0:T(8,128)(2,1)} %tok_h.1, bf16[16,1024,256]{2,1,0:T(8,128)(2,1)} %lat_h.1, bf16[16,32,1024]{2,1,0:T(8,128)(2,1)} %rope_h.1, bf16[8,128]{1,0:T(8,128)(2,1)} %bitcast.15, bf16[1024,512]{1,0:T(8,128)(2,1)} %wdq_h.1, ...), custom_call_target="tpu_custom_call" | custom-call | tf_op jit(solution)/shard_map/pallas_call | solution.py:410
  51.6 1.4 %copy.34 = bf16[16,1024]{1,0:T(8,128)(2,1)} copy(bf16[16,1024]{1,0:T(8,128)(2,1)} %get-tuple-element.4) | data formatting | bytes 65536
  53.0 1.3 %copy.35 = bf16[16,256]{1,0:T(8,128)(2,1)} copy(bf16[16,256]{1,0:T(8,128)(2,1)} %get-tuple-element.5) | data formatting | bytes 16384

commit v2 on v1

--- a/solution.py
+++ b/solution.py
@@ -18,8 +18,30 @@
 S, H, NOPE, ROPE, L, C, D = 16, 16, 64, 32, 1024, 256, 1024
 SCALE = (NOPE + ROPE) ** -0.5
 CHIPS, PLANE = 64, 16
+PART = 32
 SLOTS, QB = 4, 4
 PIECE = SLOTS * QB
+
+
+def distance(k):
+    return sum(min(d, 4 - d) for d in (k // 16, k // 4 % 4, k % 4))
+
+
+ORDER = sorted(range(1, CHIPS), key=lambda k: (-distance(k), k * 37 % 64)) + [0]
+GROUP = sorted(((kz, ky) for kz in range(4) for ky in range(4)), key=lambda k: (-distance(k[0] * 16 + k[1] * 4 + (k[0] + 2 * k[1]) % 4), k))
+GROUP.remove((0, 0))
+
+
+_open = []
+
+
+def mark(name):
+    if _open:
+        _open.pop().__exit__(None, None, None)
+    if name:
+        scope = jax.named_scope(name)
+        scope.__enter__()
+        _open.append(scope)
 
 
 def dot(a, b, dims=NN):
@@ -117,12 +139,27 @@
     tok, lat, rope, wdq, wqn, wqr, wdkv, wkr, wuk, wuv, wo, ql, qr, own_s, mixed, nlat,
     eg, eu, ed, sg, su, sd, dg, du, dd, pick, weigh,
     moe, send, recv, back, home, rows, parts, sums,
-    sems, lsem, esem, dsem, zsem_s, zsem_r, fsem_s, fsem_r, asem_s, asem_r, bsem_s, bsem_r, gsem_s, gsem_r, psem_s, psem_r,
+    sems, lsem, esem, zsem_s, zsem_r, fsem_s, fsem_r, asem_s, asem_r, bsem_s, bsem_r, gsem_s, gsem_r, psem_s, psem_r,
 ):
+    mark('start')
     ep = lax.axis_index("ep")
     tp = lax.axis_index("tp")
-    z, y, x = ep // 16, (ep // 4) % 4, ep % 4
-    plane = ep % 16
+    z, y, x = ep // 16, lax.rem(ep // 4, 4), lax.rem(ep, 4)
+    zs = [lax.rem(z + i, 4) for i in range(4)]
+    ys = [lax.rem(y + i, 4) for i in range(4)]
+    xs = [lax.rem(x + i, 4) for i in range(4)]
+    z16, y4 = [16 * v for v in zs], [4 * v for v in ys]
+    zy = z16[0] + y4[0]
+    place = 4 * z + y
+
+    def chip_of(k):
+        return z16[k // 16] + y4[k // 4 % 4] + xs[k % 4]
+
+    def chip_back(k):
+        return z16[-(k // 16) % 4] + y4[-(k // 4 % 4) % 4] + xs[-(k % 4) % 4]
+
+    def member(kz, ky):
+        return z16[kz] + y4[ky] + xs[(kz + 2 * ky) % 4], 4 * zs[kz] + ys[ky]
 
     def remote(src, dst, s_sem, r_sem, chip, core):
         return pltpu.make_async_remote_copy(
@@ -149,20 +186,16 @@
     for c in late:
         c.start()
 
+    mark('greet')
     barrier = pltpu.get_barrier_semaphore()
 
-    def chip_of(k):
-        kz, ky, kx = k // 16, (k // 4) % 4, k % 4
-        return ((z + kz) % 4) * 16 + ((y + ky) % 4) * 4 + (x + kx) % 4
-
-    def greet(k, _):
+    for k in ORDER[:-1]:
         pl.semaphore_signal(barrier, inc=1, device_id=(chip_of(k), tp), device_id_type=MESH)
-        return 0
-
-    lax.fori_loop(1, CHIPS, greet, 0)
     pl.semaphore_signal(barrier, inc=1, device_id=(ep, 1 - tp), device_id_type=MESH)
 
+    mark('tables')
     route_tables(routes, scores, pick, weigh)
+    mark('query')
 
     cosine, sine = rope_tables(len_ref)
     early[0].wait()
@@ -199,9 +232,9 @@
     own += jnp.sum(qrf.reshape(S, H, 128) * kr.astype(f32)[:, None, :], axis=-1, keepdims=True)
     own_s[...] = own.reshape(S * H, 1) * SCALE
 
+    mark('barrier')
     pl.semaphore_wait(barrier, CHIPS)
-    up_chip = ((z + 1) % 4) * 16 + plane
-    down_chip = ((z + 3) % 4) * 16 + plane
+    mark('weights_out')
     to_core = [
         remote(eg_h, eg.at[1:2], esem.at[0, 0], esem.at[1, 0], ep, 1 - tp),
         remote(eu_h, eu.at[1:2], esem.at[0, 1], esem.at[1, 1], ep, 1 - tp),
@@ -210,10 +243,12 @@
         remote(du_h, du.at[4], esem.at[0, 4], esem.at[1, 4], ep, 1 - tp),
         remote(dd_h, dd.at[4], esem.at[0, 5], esem.at[1, 5], ep, 1 - tp),
     ]
+    step = 3 - 2 * tp
+    sides = [zy + lax.rem(x + step, 4), z16[0] + 4 * lax.rem(y + step, 4) + x, 16 * lax.rem(z + step, 4) + y4[0] + x]
     to_chips = []
-    for i, (h, buf) in enumerate([(dg_h, dg), (du_h, du), (dd_h, dd)]):
-        to_chips.append(remote(h, buf.at[1], zsem_s.at[0, i], zsem_r.at[0, i], up_chip, tp))
-        to_chips.append(remote(h, buf.at[3], zsem_s.at[1, i], zsem_r.at[1, i], down_chip, tp))
+    for j in range(3):
+        for i, (h, buf) in enumerate([(dg_h, dg), (du_h, du), (dd_h, dd)]):
+            to_chips.append(remote(h, buf.at[1 + j], zsem_s.at[j, i], zsem_r.at[j, i], sides[j], tp))
     for c in to_chips + to_core:
         c.start()
 
@@ -246,7 +281,9 @@
             mixed[pl.ds(base + i * H, H)] = m.astype(bf16)
         return 0
 
+    mark('cache')
     lax.fori_loop(0, 4, group, 0)
+    mark('attn_out')
     late[0].wait()
     full = dot(mixed[...], wuv[...]).reshape(S, H, D)
     ho = jnp.sum(jnp.where(head[None], full, 0.0), axis=1).astype(bf16)
@@ -255,43 +292,34 @@
     moe_in = rms(first.astype(f32), row_of(mg)).astype(bf16)
     moe[...] = moe_in
 
+    mark('pack')
     blocks = jnp.concatenate([moe_in[:, 256 * q : 256 * q + 256] for q in range(QB)], axis=0)
     send[...] = dot(pick[...], blocks).astype(bf16).reshape(CHIPS, PIECE, 256)
-    recv[ep] = send[ep]
-    rows[plane] = moe_in
-
-    def dispatch(k, _):
+    recv[CHIPS - 1] = send[ep]
+    rows[place] = moe_in
+    mark('dispatch')
+    for i, k in enumerate(ORDER[:-1]):
         chip = chip_of(k)
-        remote(send.at[chip], recv.at[ep], asem_s, asem_r.at[k // 16], chip, tp).start()
-        return 0
-
-    def gather(k, _):
-        chip = chip_of(k)
-        remote(moe, rows.at[plane], gsem_s, gsem_r, chip, tp).start()
-        return 0
-
-    lax.fori_loop(1, CHIPS, dispatch, 0)
-    lax.fori_loop(1, PLANE, gather, 0)
-
-    for i, buf in enumerate([dg, du, dd]):
-        remote(buf.at[1], buf.at[1], zsem_s.at[0, i], zsem_r.at[0, i], up_chip, tp).wait_recv()
-        remote(buf.at[3], buf.at[3], zsem_s.at[1, i], zsem_r.at[1, i], down_chip, tp).wait_recv()
-    onward = jnp.where(tp == 0, 1, 3)
-    next_chip = jnp.where(tp == 0, up_chip, down_chip)
-    onwards, crossing = [], []
-    for i, buf in enumerate([dg, du, dd]):
-        onwards.append(remote(buf.at[onward], buf.at[2], fsem_s.at[0, i], fsem_r.at[0, i], next_chip, tp))
-    for i, buf in enumerate([dg, du, dd]):
-        crossing.append(remote(buf.at[1], buf.at[5], fsem_s.at[1, i], fsem_r.at[1, i], ep, 1 - tp))
-        crossing.append(remote(buf.at[3], buf.at[7], fsem_s.at[2, i], fsem_r.at[2, i], ep, 1 - tp))
-    for c in onwards + crossing:
+        remote(send.at[chip], recv.at[i], asem_s, asem_r.at[i // PART], chip, tp).start()
+    for k in GROUP:
+        remote(moe, rows.at[place], gsem_s, gsem_r, member(*k)[0], tp).start()
+
+    mark('onward')
+    crossing = []
+    for j in range(3):
+        for i, buf in enumerate([dg, du, dd]):
+            to_chips[3 * j + i].wait_recv()
+            crossing.append(remote(buf.at[1 + j], buf.at[5 + j], fsem_s.at[j, i], fsem_r.at[j, i], ep, 1 - tp))
+    for c in crossing:
         c.start()
 
+    mark('shared')
     for c in late[5:8]:
         c.wait()
     shared_act = (silu(dot(moe_in, sg[...])) * dot(moe_in, su[...])).astype(bf16)
     mixture = dot(shared_act, sd[...])
 
+    mark('expert_w')
     for c in late[2:5]:
         c.wait()
     for c in to_core[0:3]:
@@ -299,79 +327,83 @@
     m, n = iota((256, 256), 0), iota((256, 256), 1)
     sort = ((m // 64 == (n // SLOTS) % QB) & ((m % 64) // SLOTS == n // PIECE) & (m % SLOTS == n % SLOTS))
     sort = jnp.where(sort, 1.0, 0.0).astype(bf16)
-    for i in range(4):
-        g = (z + 4 - i) % 4
-        lo = pl.multiple_of(g * PLANE, PLANE)
-        if i == 0:
-            pltpu.make_async_copy(recv.at[0:15], recv.at[0:15], asem_r.at[0]).wait()
-        else:
-            pltpu.make_async_copy(recv.at[0:16], recv.at[0:16], asem_r.at[i]).wait()
-        got = dot(sort, recv[pl.ds(lo, PLANE)].reshape(PLANE * PIECE, 256)).astype(bf16)
-        rows_in = jnp.concatenate([got[64 * q : 64 * q + 64] for q in range(QB)], axis=1)
-        total = jnp.zeros((64, D), f32)
+    for g in range(CHIPS // PART):
+        mark('expert_wait')
+        lo, others = g * PART, PART - (g == CHIPS // PART - 1)
+        pltpu.make_async_copy(recv.at[0:others], recv.at[0:others], asem_r.at[g]).wait()
+        mark('expert')
+        rows_in = []
+        for h in range(lo, lo + PART, PLANE):
+            got = dot(sort, recv[h : h + PLANE].reshape(PLANE * PIECE, 256)).astype(bf16)
+            rows_in.append(jnp.concatenate([got[64 * q : 64 * q + 64] for q in range(QB)], axis=1))
+        rows_in = jnp.concatenate(rows_in, axis=0)
+        total = jnp.zeros((PART * SLOTS, D), f32)
         for part in range(2):
             act = (silu(dot(rows_in, eg[part])) * dot(rows_in, eu[part])).astype(bf16)
             total += dot(act, ed[part]).astype(bf16).astype(f32)
         total = total.astype(bf16)
-        total = jnp.concatenate([total[:, 256 * q : 256 * q + 256] for q in range(QB)], axis=0)
-        back[pl.ds(lo, PLANE)] = dot(sort, total, TN).astype(bf16).reshape(PLANE, PIECE, 256)
-        if i == 0:
-            home[ep] = back[ep]
-
-        def give(k, _):
-            chip = chip_of(((4 - i) % 4) * 16 + k)
-            remote(back.at[chip], home.at[ep], bsem_s, bsem_r, chip, tp).start()
-            return 0
-
-        lax.fori_loop(1 if i == 0 else 0, PLANE, give, 0)
-
-    for c in onwards:
-        c.wait_recv()
-    last = [
-        remote(buf.at[2], buf.at[6], fsem_s.at[3, i], fsem_r.at[3, i], ep, 1 - tp) for i, buf in enumerate([dg, du, dd])
-    ]
-    for c in last:
-        c.start()
+        for j, h in enumerate(range(lo, lo + PART, PLANE)):
+            some = total[64 * j : 64 * j + 64]
+            some = jnp.concatenate([some[:, 256 * q : 256 * q + 256] for q in range(QB)], axis=0)
+            back[h : h + PLANE] = dot(sort, some, TN).astype(bf16).reshape(PLANE, PIECE, 256)
+        mark('give')
+        for i in range(lo, lo + others):
+            remote(back.at[i], home.at[ep], bsem_s, bsem_r, chip_back(ORDER[i]), tp).start()
+    home[ep] = back[CHIPS - 1]
+
+    mark('dense_w')
     for c in late[8:11]:
         c.wait()
-    for c in to_core[3:6] + crossing + last:
+    for c in to_core[3:6] + crossing:
         c.wait_recv()
     pltpu.make_async_copy(rows.at[0:15], rows.at[0:15], gsem_r).wait()
+    mark('dense')
     all_rows = rows[...].reshape(PLANE * S, D)
     gate_h = dot(all_rows, dg[...].reshape(512, D), NT)
     up_h = dot(all_rows, du[...].reshape(512, D), NT)
     act = (silu(gate_h) * up_h).astype(bf16)
     parts[...] = dot(act, dd[...].reshape(512, D)).astype(bf16).reshape(PLANE, S, D)
-    sums[plane] = parts[plane]
-
-    def share(k, _):
-        chip = chip_of(k)
-        remote(parts.at[chip % 16], sums.at[plane], psem_s, psem_r, chip, tp).start()
-        return 0
-
-    lax.fori_loop(1, PLANE, share, 0)
+    sums[place] = parts[place]
+    mark('share')
+    for k in GROUP:
+        chip, its = member(*k)
+        remote(parts.at[its], sums.at[place], psem_s, psem_r, chip, tp).start()
 
     gate = jnp.sum(moe_in.astype(f32) * row_of(dvec), axis=-1, keepdims=True)
     gate = 1.0 / (1.0 + jnp.exp(-gate))
 
+    mark('home_wait')
     pltpu.make_async_copy(home.at[0:63], home.at[0:63], bsem_r).wait()
+    mark('routed')
     routed = dot(weigh[...], home[...].reshape(CHIPS * PIECE, 256))
     routed = routed[0:64] + routed[64:128]
     mixture += jnp.concatenate([routed[S * q : S * q + S] for q in range(QB)], axis=1)
 
+    mark('sums_wait')
     pltpu.make_async_copy(sums.at[0:15], sums.at[0:15], psem_r).wait()
+    mark('final')
     dense = jnp.zeros((S, D), f32)
     for p in range(PLANE):
         dense += sums[p].astype(f32)
     mixture += gate * dense
     out_o[...] = (first.astype(f32) + rms(mixture, row_of(og))).astype(bf16)
 
-    for c in to_chips + to_core + onwards + crossing + last:
+    mark('drain')
+    for c in to_chips + to_core + crossing:
         c.wait_send()
     pltpu.make_async_copy(send.at[0:63], send.at[0:63], asem_s).wait()
     pltpu.make_async_copy(back.at[0:63], back.at[0:63], bsem_s).wait()
     pltpu.make_async_copy(rows.at[0:15], rows.at[0:15], gsem_s).wait()
     pltpu.make_async_copy(parts.at[0:15], parts.at[0:15], psem_s).wait()
+    mark(None)
+
+
+def put_out(a, b, a_o, b_o, sems):
+    copies = [pltpu.make_async_copy(a, a_o, sems.at[0]), pltpu.make_async_copy(b, b_o, sems.at[1])]
+    for c in copies:
+        c.start()
+    for c in copies:
+        c.wait()
 
 
 def step(
@@ -404,12 +436,12 @@
         v(2, 1024, 256), v(2, 1024, 256), v(2, 256, 1024), v(1024, 512), v(1024, 512), v(512, 1024),
         v(8, 64, 1024), v(8, 64, 1024), v(8, 64, 1024), v(1024, 64), v(128, 1024),
         v(16, 1024), v(64, 16, 256), v(64, 16, 256), v(64, 16, 256), v(64, 16, 256), v(16, 16, 1024), v(16, 16, 1024), v(16, 16, 1024),
-        dma((18,)), dma((4, 2)), dma((2, 6)), dma((1,)), dma((2, 3)), dma((2, 3)), dma((4, 3)), dma((4, 3)),
-        dma, dma((4,)), dma, dma, dma, dma, dma, dma,
+        dma((18,)), dma((4, 2)), dma((2, 6)), dma((3, 3)), dma((3, 3)), dma((3, 3)), dma((3, 3)),
+        dma, dma((CHIPS // PART,)), dma, dma, dma, dma, dma, dma,
     ]
-    return pl.pallas_call(
+    results = pl.pallas_call(
         kernel,
-        out_shape=[jax.ShapeDtypeStruct((S, D), bf16), jax.ShapeDtypeStruct((S, C), bf16)],
+        out_shape=[pltpu.VMEM((S, D), bf16), pltpu.VMEM((S, C), bf16)],
         in_specs=[s for _, s in operands],
         out_specs=[vm, vm],
         scratch_shapes=scratch,
@@ -417,6 +449,13 @@
             collective_id=0, has_side_effects=True, vmem_limit_bytes=62 * 2**20
         ),
     )(*[a for a, _ in operands])
+    return pl.pallas_call(
+        put_out,
+        out_shape=[jax.ShapeDtypeStruct((S, D), bf16), jax.ShapeDtypeStruct((S, C), bf16)],
+        in_specs=[vm, vm],
+        out_specs=[anyspec, anyspec],
+        scratch_shapes=[dma((2,))],
+    )(*[pltpu.with_memory_space_constraint(r, pltpu.VMEM) for r in results])
 
 
 def solution(mesh):

time: 54.5 us -> 44 us (0.81)
  Pallas kernels: 50.9 us -> 43.1 us
  local copies, waits for them, and re-layouts: 2.67 us -> 0 us
    pallas_call x1 -> x2, Pallas kernels: 50.9 us -> 43.1 us  [the longest x1 42.5 us: step(): pl.pallas_call(kernel, out_shape=[pltpu.VMEM((S, D), bf16), pltpu.VMEM((S...]
    unnamed x2 -> x0, local copies, waits for them, and re-layouts: 2.67 us -> none
where the time goes in v2:
time: 44 us; the launch traced here: 43.8 us
  Pallas kernels  43.1 us (98%)
  between operations  0.65 us (1%)
    pallas_call x1, Pallas kernels, step(): pl.pallas_call(kernel, out_shape=[pltpu.VMEM((S, D), bf16), pltpu.VMEM((S...  42.5 us

profile of v2, /device:TPU:1, one launch (start us, length us, event | category | flops | bytes accessed | tf_op | source)
XLA Modules:
  0.0 43.8 jit_solution(12072922609016555138)
XLA Ops:
  0.6 42.5 %shard_map.293 = (bf16[16,1024]{1,0:T(8,128)(2,1)S(1)}, bf16[16,256]{1,0:T(8,128)(2,1)S(1)}) custom-call(s32[16]{0:T(128)} %len_ref.1, bf16[16,1024]{1,0:T(8,128)(2,1)} %tok_h.1, bf16[16,1024,256]{2,1,0:T(8,128)(2,1)} %lat_h.1, bf16[16,32,1024]{2,1,0:T(8,128)(2,1)} %rope_h.1, bf16[8,128]{1,0:T(8,128)(2,1)} %bitcast.15, bf16[1024,512]{1,0:T(8,128)(2,1)} %wdq_h.1, ...), custom_call_target="tpu_custom_call" | custom-call | tf_op jit(solution)/shard_map/pallas_call | solution.py:442
  43.1 0.6 %shard_map.294 = (bf16[16,1024]{1,0:T(8,128)(2,1)}, bf16[16,256]{1,0:T(8,128)(2,1)}) custom-call(bf16[16,1024]{1,0:T(8,128)(2,1)S(1)} %get-tuple-element.4.a, bf16[16,256]{1,0:T(8,128)(2,1)S(1)} %get-tuple-element.5.b), custom_call_target="tpu_custom_call" | custom-call | tf_op jit(solution)/shard_map/pallas_call | solution.py:452
